TPU v7x, 32 devices: a whole 2x2x4 slice. The times are simulated.
32 devices in a mesh: row: 8 (over z, x), col: 4 (over y, core).
Axes of the slice: x: 2, y: 2, z: 4, core: 2. Of those that a mesh axis runs over, the one named last changes fastest.
Arguments:
- tokens: bfloat16 [2, 32768, 2048], P(None, ('row', 'col')), may hold values from -6 to 6
- norm_gain: float32 [2048], replicated, may hold values from 0.1 to 1.9
- mix_weight: bfloat16 [2048, 1024], replicated, may hold values from -0.125 to 0.125
- gate_weight: bfloat16 [2048, 2048], replicated, may hold values from -0.125 to 0.125
- out_weight: bfloat16 [1024, 2048], replicated, may hold values from -0.1875 to 0.1875
Outputs:
- gated: bfloat16 [2, 32768, 2048], P(None, ('row', 'col'))
All inputs are finite; a program needn't handle non-finite values.
Results may differ from a plain program's by a relative error of at most 0.017.
Values may be sent and summed in bfloat16 or wider, within the bound.
A program may use at most 128 MiB of HBM per device.

v0:
```python
import math

import jax
import jax.numpy as jnp
from jax import lax
from jax.sharding import PartitionSpec as P

GROUP_DIM = 128
LEN1 = 128


def tables(length, factor):
    indices = jnp.arange(length, dtype=jnp.int32)
    products = indices[:, None] * indices[None, :] % length
    angles = products.astype(jnp.float32) * (2.0 * math.pi / length)
    return (jnp.cos(angles) * factor, jnp.sin(angles) * factor)


def length_transform(values, first_span):
    item_count, span_total, column_count = values.shape
    second_span = span_total // first_span
    highest = lax.Precision.HIGHEST
    cos_first, sin_first = tables(first_span, span_total ** (-0.5))
    cos_second, sin_second = tables(second_span, 1.0)
    row_index = jnp.arange(first_span, dtype=jnp.int32)[:, None]
    col_index = jnp.arange(second_span, dtype=jnp.int32)[None, :]
    twist_angle = (row_index * col_index % span_total).astype(jnp.float32) * (
        2.0 * math.pi / span_total
    )
    twist_cos = jnp.cos(twist_angle)[None, :, :, None]
    twist_sin = jnp.sin(twist_angle)[None, :, :, None]
    arranged = values.reshape(item_count, first_span, second_span, column_count)
    part_real = jnp.einsum("ka,sabc->skbc", cos_first, arranged, precision=highest)
    part_imaginary = -jnp.einsum("ka,sabc->skbc", sin_first, arranged, precision=highest)
    turned_real = part_real * twist_cos + part_imaginary * twist_sin
    turned_imaginary = part_imaginary * twist_cos - part_real * twist_sin
    real_part = jnp.einsum(
        "skbc,bm->smkc", turned_real, cos_second, precision=highest
    ) + jnp.einsum("skbc,bm->smkc", turned_imaginary, sin_second, precision=highest)
    imaginary = jnp.einsum(
        "skbc,bm->smkc", turned_imaginary, cos_second, precision=highest
    ) - jnp.einsum("skbc,bm->smkc", turned_real, sin_second, precision=highest)
    return (
        real_part.reshape(item_count, span_total, column_count),
        imaginary.reshape(item_count, span_total, column_count),
    )


def local(tokens, norm_gain, mix_weight, gate_weight, out_weight):
    widened = tokens.astype(jnp.float32)
    inverse_rms = lax.rsqrt(jnp.mean(widened * widened, axis=-1, keepdims=True) + 1e-06)
    normed = (widened * inverse_rms * norm_gain).astype(jnp.bfloat16)
    mixed_in = jnp.dot(normed, mix_weight, preferred_element_type=jnp.float32).astype(jnp.bfloat16)
    half_dim = GROUP_DIM // 2
    cos_group, sin_group = tables(GROUP_DIM, GROUP_DIM ** (-0.5))
    left_table = cos_group[:, :half_dim]
    right_table = jnp.concatenate(
        [cos_group[:, half_dim : half_dim + 1], sin_group[:, 1:half_dim]], axis=1
    )
    incoming = lax.all_to_all(mixed_in, "col", split_axis=2, concat_axis=1, tiled=True)
    item_count = incoming.shape[0]
    row_count = incoming.shape[1]
    grouped = incoming.astype(jnp.float32).reshape(item_count, row_count, -1, GROUP_DIM)
    left_part = jnp.einsum("srgj,jk->srgk", grouped, left_table, precision=lax.Precision.HIGHEST)
    right_part = jnp.einsum("srgj,jk->srgk", grouped, right_table, precision=lax.Precision.HIGHEST)
    spectra = jnp.stack(
        [
            left_part.reshape(item_count, row_count, -1),
            right_part.reshape(item_count, row_count, -1),
        ],
        axis=2,
    )
    gate_value = jax.nn.sigmoid(jnp.dot(normed, gate_weight, preferred_element_type=jnp.float32))
    seq_count, block_rows = (spectra.shape[0], spectra.shape[1])
    pair_width = spectra.shape[3] // lax.axis_size("row")
    flat_index = lax.axis_index("row") * pair_width + jnp.arange(pair_width, dtype=jnp.int32)
    lone_pair = flat_index % half_dim == 0
    stacked = lax.all_to_all(
        spectra.astype(jnp.bfloat16), "row", split_axis=3, concat_axis=1, tiled=True
    ).astype(spectra.dtype)
    width_here = stacked.shape[3]
    joined_in = jnp.concatenate([stacked[:, :, 0], stacked[:, :, 1]], axis=2)
    real_part, imaginary = length_transform(joined_in, LEN1)
    sum_pair = real_part[..., :width_here] + imaginary[..., width_here:]
    diff_pair = real_part[..., :width_here] - imaginary[..., width_here:]
    lower_half = jnp.where(lone_pair, real_part[..., :width_here], sum_pair).astype(jnp.bfloat16)
    upper_half = jnp.where(lone_pair, real_part[..., width_here:], diff_pair).astype(jnp.bfloat16)
    both_halves = jnp.stack([lower_half, upper_half], axis=2)
    returned = lax.all_to_all(both_halves, "row", split_axis=1, concat_axis=3, tiled=True)
    lower_half = returned[:, :, 0].reshape(seq_count, block_rows, -1, half_dim)
    upper_half = returned[:, :, 1].reshape(seq_count, block_rows, -1, half_dim)
    spectral = jnp.concatenate(
        [lower_half, upper_half[..., :1], jnp.flip(upper_half[..., 1:], axis=3)], axis=3
    )
    spectral = spectral.reshape(seq_count, block_rows, -1)
    spectral_rows = lax.all_to_all(spectral, "col", split_axis=1, concat_axis=2, tiled=True)
    mapped = jnp.dot(spectral_rows, out_weight, preferred_element_type=jnp.float32)
    return (gate_value * mapped).astype(jnp.bfloat16)


def solution(mesh):
    in_specs = (P(None, ("row", "col"), None), P(), P(), P(), P())
    out_specs = P(None, ("row", "col"), None)
    return jax.shard_map(local, mesh=mesh, in_specs=in_specs, out_specs=out_specs, check_vma=False)
```

profile of v0, /device:TPU:0, one launch (start us, length us, event | category | flops | bytes accessed | tf_op | source)
XLA Modules:
  0.0 793.8 jit_solution(2440086694981765135)
XLA Ops:
  5.9 12.8 %fusion.21 = bf16[2,1024,1024]{2,1,0:T(8,128)(2,1)} fusion(bf16[2048,1024]{1,0:T(8,128)(2,1)} %param.7, bf16[2,1024,2048]{2,1,0:T(8,128)(2,1)S(1)} %copy-done.5, f32[2048]{0:T(1024)S(1)} %copy-done.9, f32[2,1024]{1,0:T(2,128)S(1)} %add_rsqrt_fusion), kind=kOutput, calls=%fused_computation.35 | convolution fusion | flops 8608808960 | bytes 16793600 | tf_op jit(solution)/shard_map/dot_general | solution.py:53
  18.7 11.4 %copy.68 = bf16[2,1024,1024]{1,0,2:T(2,128)(2,1)} copy(bf16[2,1024,1024]{2,1,0:T(8,128)(2,1)} %fusion.21) | data formatting | bytes 8388608 | tf_op jit(solution)/shard_map/convert_element_type | solution.py:53
  35.5 48.3 %all-to-all-done = bf16[2,1024,1024]{1,0,2:T(2,128)(2,1)} async-done(((bf16[2,1024,1024]{1,0,2:T(2,128)(2,1)}), bf16[2,1024,1024]{1,0,2:T(2,128)(2,1)}, u32[]{:S(2)}, u32[]{:S(2)}) %all-to-all-start) | async-done | bytes 4194336 | tf_op jit(solution)/shard_map/all_to_all | solution.py:60
  83.8 11.1 %copy.69 = bf16[2,1024,4,256]{3,1,2,0:T(8,128)(2,1)} copy(bf16[2,1024,4,256]{1,0,3,2:T(2,128)(2,1)} %bitcast.4) | data formatting | bytes 8388608 | tf_op jit(solution)/shard_map/all_to_all | solution.py:60
  94.9 7.0 reshape.69
  101.9 8.1 %convolution_convert_fusion.1 = bf16[2,4096,2,64]{1,3,2,0:T(8,128)(2,1)} fusion(bf16[2,4096,2,128]{3,2,1,0:T(2,128)(2,1)} %reshape.69, f32[128,128]{0,1:T(8,128)S(1)} %broadcast_multiply_fusion), kind=kOutput, calls=%fused_computation.23 | convolution fusion | flops 1611661312 | bytes 6324224 | tf_op jit(solution)/shard_map/srgj,jk->srgk/dot_general | solution.py:64
  110.0 6.4 copy.72
  116.4 5.8 convolution_convert_fusion
  122.2 6.6 copy.73
  128.8 10.5 %pad_maximum_fusion.3 = bf16[2,4096,2,128]{1,2,0,3:T(2,128)(2,1)} fusion(bf16[2,4096,1,128]{1,2,0,3:T(2,128)(2,1)S(1)} %copy.73, bf16[2,4096,1,128]{1,2,0,3:T(2,128)(2,1)S(1)} %copy.72), kind=kLoop, calls=%fused_computation.27 | loop fusion | flops 8388608 | bytes 8388608 | tf_op jit(solution)/shard_map/stack | solution.py:66
  139.3 6.6 all-to-all-start.1
  146.5 92.4 %all-to-all-done.1 = bf16[2,4096,2,128]{1,2,0,3:T(2,128)(2,1)} async-done(((bf16[2,4096,2,128]{1,2,0,3:T(2,128)(2,1)}), bf16[2,4096,2,128]{1,2,0,3:T(2,128)(2,1)}, u32[]{:S(2)}, u32[]{:S(2)}) %all-to-all-start.1) | async-done | bytes 4194336 | tf_op jit(solution)/shard_map/all_to_all | solution.py:78
  257.3 5.5 copy.107
  268.1 9.9 %fusion.9 = f32[2,256,32,128]{3,1,2,0:T(8,128)S(1)} fusion(f32[2,128,256,16]{1,2,3,0:T(8,128)} %copy.77, f32[2,128,256,16]{1,2,3,0:T(8,128)} %copy.76), kind=kOutput, calls=%fused_computation.18 | convolution fusion | flops 3223568384 | bytes 16777216 | tf_op jit(solution)/shard_map/ka,sabc->skbc/dot_general | solution.py:34
  278.0 9.2 %fusion.10 = f32[2,256,32,128]{3,1,2,0:T(8,128)S(1)} fusion(f32[2,128,256,16]{1,2,3,0:T(8,128)S(1)} %copy-done.4, f32[2,128,256,16]{1,2,3,0:T(8,128)S(1)} %copy-done.3), kind=kOutput, calls=%fused_computation.19 | convolution fusion | flops 3223568384 | bytes 16777216 | tf_op jit(solution)/shard_map/ka,sabc->skbc/dot_general | solution.py:33
  287.3 12.1 %fusion.28 = f32[256,2,128,32]{2,0,3,1:T(8,128)} fusion(f32[2,256,32,128]{3,1,2,0:T(8,128)S(1)} %fusion.10, f32[2,256,32,128]{3,1,2,0:T(8,128)S(1)} %fusion.9, f32[128,256]{0,1:T(8,128)S(1)} %get-tuple-element.11, f32[128,256]{0,1:T(8,128)S(1)} %get-tuple-element.12), kind=kOutput, calls=%fused_computation.38 | convolution fusion | flops 6451757056 | bytes 25427968 | tf_op jit(solution)/shard_map/skbc,bm->smkc/dot_general | solution.py:40
  299.4 12.2 %fusion.32 = f32[256,2,128,32]{2,0,3,1:T(8,128)} fusion(f32[2,256,32,128]{3,1,2,0:T(8,128)S(1)} %fusion.10, f32[2,256,32,128]{3,1,2,0:T(8,128)S(1)} %fusion.9, f32[128,256]{0,1:T(8,128)S(1)} %get-tuple-element.11, f32[128,256]{0,1:T(8,128)S(1)} %get-tuple-element.12), kind=kOutput, calls=%fused_computation.39 | convolution fusion | flops 6451757056 | bytes 25427968 | tf_op jit(solution)/shard_map/skbc,bm->smkc/dot_general | solution.py:37
  311.6 19.3 %subtract_bitcast_fusion = f32[2,256,128,32]{2,1,3,0:T(8,128)} fusion(f32[256,2,128,32]{2,0,3,1:T(8,128)} %fusion.28, f32[2,256,32,128]{3,1,2,0:T(8,128)} %copy-done.1, f32[2,256,32,128]{3,1,2,0:T(8,128)S(1)} %fusion.9, f32[128,256]{0,1:T(8,128)S(1)} %get-tuple-element.11, f32[128,256]{0,1:T(8,128)S(1)} %get-tuple-element.12), kind=kOutput, calls=%fused_computation.16 | convolution fusion | flops 6453854208 | bytes 33816576 | tf_op jit(solution)/shard_map/skbc,bm->smkc/dot_general | solution.py:42
  330.9 9.4 %reshape.71 = f32[2,32768,32]{1,2,0:T(8,128)} reshape(f32[2,256,128,32]{2,1,3,0:T(8,128)} %subtract_bitcast_fusion) | data formatting | bytes 16777216 | tf_op jit(solution)/shard_map/reshape | solution.py:45
  340.3 22.0 %add_bitcast_fusion = f32[2,256,128,32]{2,1,3,0:T(8,128)} fusion(f32[256,2,128,32]{2,0,3,1:T(8,128)} %fusion.32, f32[2,256,32,128]{3,1,2,0:T(8,128)} %copy-done.1, f32[2,256,32,128]{3,1,2,0:T(8,128)} %copy-done, f32[128,256]{0,1:T(8,128)S(1)} %get-tuple-element.11, f32[128,256]{0,1:T(8,128)S(1)} %get-tuple-element.12), kind=kOutput, calls=%fused_computation.17 | convolution fusion | flops 6453854208 | bytes 33816576 | tf_op jit(solution)/shard_map/skbc,bm->smkc/dot_general | solution.py:39
  362.4 9.4 %reshape.70 = f32[2,32768,32]{1,2,0:T(8,128)} reshape(f32[2,256,128,32]{2,1,3,0:T(8,128)} %add_bitcast_fusion) | data formatting | bytes 16777216 | tf_op jit(solution)/shard_map/reshape | solution.py:44
  371.7 5.5 fusion.27
  379.6 62.0 %copy.84 = bf16[2,32768,2,16]{3,2,0,1:T(2,128)(2,1)} copy(bf16[2,32768,2,16]{1,3,2,0:T(8,128)(2,1)} %pad_maximum_fusion.4) | data formatting | bytes 8388608 | tf_op jit(solution)/shard_map/stack | solution.py:88
  441.6 37.9 %reshape.84 = bf16[8,2,131072]{2,1,0:T(2,128)(2,1)} reshape(bf16[32768,2,2,16]{3,2,1,0:T(2,128)(2,1)} %bitcast.123) | data formatting | bytes 8388608
  479.5 97.3 %all_to_all.60 = bf16[8,2,131072]{2,1,0:T(2,128)(2,1)} all-to-all(bf16[8,2,131072]{2,1,0:T(2,128)(2,1)} %reshape.84), channel_id=1, replica_groups=mesh['row'=8,'col'=4] {'row'}, dimensions={0} | all-to-all | bytes 8388608 | tf_op jit(solution)/shard_map/all_to_all | solution.py:89
  576.8 25.8 %reshape.85 = bf16[32768,2,2,16]{3,2,1,0:T(2,128)(2,1)} reshape(bf16[8,2,131072]{2,1,0:T(2,128)(2,1)} %all_to_all.60) | data formatting | bytes 8388608
  602.6 67.5 %copy.103 = bf16[2,8,4096,2,16]{2,4,1,3,0:T(8,128)(2,1)} copy(bf16[2,8,4096,2,16]{4,3,0,2,1:T(2,128)(2,1)} %bitcast.124) | data formatting | bytes 8388608 | tf_op jit(solution)/shard_map/all_to_all | solution.py:89
  674.7 11.4 %rev.4 = bf16[2,4096,2,63]{1,3,2,0:T(8,128)(2,1)} reverse(bf16[2,4096,2,63]{1,3,2,0:T(8,128)(2,1)S(1)} %slice.62), dimensions={3} | reverse | bytes 4128768 | tf_op jit(solution)/shard_map/jit(_flip)/rev | solution.py:93
  690.1 11.1 %copy.87 = bf16[2,4096,256]{2,0,1:T(2,128)(2,1)} copy(bf16[2,4096,256]{1,2,0:T(8,128)(2,1)} %bitcast.128) | data formatting | bytes 8388608 | tf_op jit(solution)/shard_map/reshape | solution.py:95
  701.2 52.2 %all_to_all.61 = bf16[2,4096,256]{2,0,1:T(2,128)(2,1)S(1)} all-to-all(bf16[2,4096,256]{2,0,1:T(2,128)(2,1)} %copy.87), channel_id=1, replica_groups=mesh['row'=8,'col'=4] {'col'}, dimensions={1} | all-to-all | bytes 8388608 | tf_op jit(solution)/shard_map/all_to_all | solution.py:96
  755.6 11.7 %fusion.16 = f32[2,1024,2048]{2,1,0:T(8,128)} fusion(bf16[2,1024,1024]{2,1,0:T(8,128)(2,1)S(1)} %bitcast.142, bf16[1024,2048]{1,0:T(8,128)(2,1)S(1)} %copy-done.8), kind=kOutput, calls=%fused_computation.30 | convolution fusion | flops 8589934592 | bytes 25165824 | tf_op jit(solution)/shard_map/dot_general | solution.py:97
  767.3 26.0 %multiply_convert_fusion = bf16[2,1024,2048]{2,1,0:T(8,128)(2,1)} fusion(f32[2,1024,2048]{2,1,0:T(8,128)} %fusion.16, bf16[2048,2048]{1,0:T(8,128)(2,1)} %param.8, bf16[2,1024,2048]{2,1,0:T(8,128)(2,1)S(1)} %bitcast.140, f32[2048]{0:T(1024)S(1)} %copy-done.10, f32[2,1024]{1,0:T(2,128)S(1)} %copy-done.7), kind=kOutput, calls=%fused_computation.5 | convolution fusion | flops 17217617920 | bytes 41959424 | tf_op jit(solution)/shard_map/dot_general | solution.py:73
  (50 shorter events, 48.6 us)
Async XLA Ops:
  0.0 5.9 copy-start.5
  0.0 5.9 copy-start.9
  5.3 0.6 copy-start.6
  30.0 53.8 %all-to-all-start = ((bf16[2,1024,1024]{1,0,2:T(2,128)(2,1)}), bf16[2,1024,1024]{1,0,2:T(2,128)(2,1)}, u32[]{:S(2)}, u32[]{:S(2)}) async-start(bf16[2,1024,1024]{1,0,2:T(2,128)(2,1)} %copy.68), calls=%async_computation | async-start | bytes 8388608 | tf_op jit(solution)/shard_map/all_to_all | solution.py:60
  101.9 14.5 %copy-start.2 = (bf16[2,4096,2,128]{3,2,1,0:T(2,128)(2,1)S(1)}, bf16[2,4096,2,128]{3,2,1,0:T(2,128)(2,1)}, u32[]{:S(2)}) copy-start(bf16[2,4096,2,128]{3,2,1,0:T(2,128)(2,1)} %reshape.69) | copy-start | bytes 12582916
  139.3 99.6 %all-to-all-start.1 = ((bf16[2,4096,2,128]{1,2,0,3:T(2,128)(2,1)}), bf16[2,4096,2,128]{1,2,0,3:T(2,128)(2,1)}, u32[]{:S(2)}, u32[]{:S(2)}) async-start(bf16[2,4096,2,128]{1,2,0,3:T(2,128)(2,1)} %pad_maximum_fusion.3), calls=%async_computation.1 | async-start | bytes 8388608 | tf_op jit(solution)/shard_map/all_to_all | solution.py:78
  268.1 10.0 %copy-start.3 = (f32[2,128,256,16]{1,2,3,0:T(8,128)S(1)}, f32[2,128,256,16]{1,2,3,0:T(8,128)}, u32[]{:S(2)}) copy-start(f32[2,128,256,16]{1,2,3,0:T(8,128)} %copy.76) | copy-start | bytes 12582916
  268.1 10.0 %copy-start.4 = (f32[2,128,256,16]{1,2,3,0:T(8,128)S(1)}, f32[2,128,256,16]{1,2,3,0:T(8,128)}, u32[]{:S(2)}) copy-start(f32[2,128,256,16]{1,2,3,0:T(8,128)} %copy.77) | copy-start | bytes 12582916
  278.0 33.6 %copy-start = (f32[2,256,32,128]{3,1,2,0:T(8,128)}, f32[2,256,32,128]{3,1,2,0:T(8,128)S(1)}, u32[]{:S(2)}) copy-start(f32[2,256,32,128]{3,1,2,0:T(8,128)S(1)} %fusion.9) | copy-start | bytes 25165828
  287.2 12.2 %copy-start.1 = (f32[2,256,32,128]{3,1,2,0:T(8,128)}, f32[2,256,32,128]{3,1,2,0:T(8,128)S(1)}, u32[]{:S(2)}) copy-start(f32[2,256,32,128]{3,1,2,0:T(8,128)S(1)} %fusion.10) | copy-start | bytes 25165828
  753.4 2.2 copy-start.8
  754.0 13.4 %slice-start = ((s8[8388608]{0:T(1024)(128)(4,1)}), s8[4194304]{0:T(1024)(128)(4,1)S(1)}, s32[]{:S(2)}) async-start(s8[8388608]{0:T(1024)(128)(4,1)} %bitcast.139), calls=%async_computation.4 | async-start | bytes 8388608
  755.6 11.7 %slice-start.1 = ((s8[8388608]{0:T(1024)(128)(4,1)}), s8[4194304]{0:T(1024)(128)(4,1)S(1)}, s32[]{:S(2)}) async-start(s8[8388608]{0:T(1024)(128)(4,1)} %bitcast.139), calls=%async_computation.5 | async-start | bytes 8388608
  755.6 11.7 %copy-start.7 = (f32[2,1024]{1,0:T(2,128)S(1)}, f32[2,1024]{1,0:T(2,128)}, u32[]{:S(2)}) copy-start(f32[2,1024]{1,0:T(2,128)} %copy-done.6) | copy-start | bytes 24580
  755.6 11.7 %copy-start.10 = (f32[2048]{0:T(1024)S(1)}, f32[2048]{0:T(1024)}, u32[]{:S(2)}) copy-start(f32[2048]{0:T(1024)} %param.6) | copy-start | bytes 24580
where the time goes:
time: 809 us; the launch traced here: 794 us
  local copies, waits for them, and re-layouts  312 us (39%)
  matrix products  149 us (18%)
  blocking collectives  149 us (18%)
  waiting for transfers between devices  141 us (17%)
  other arithmetic  29.8 us (4%)
  starting transfers between devices  11.4 us (1%)
    all_to_all x1, blocking collectives, local(): lax.all_to_all(both_halves, 'row', split_axis=1, concat_axis=3, tiled=True)  97.3 us
    all_to_all x1, waiting for transfers between devices, local(): lax.all_to_all(spectra.astype(jnp.bfloat16), 'row', split_axis=3, concat_...  92.4 us
    unnamed x30, local copies, waits for them, and re-layouts  74.1 us
    all_to_all x1, local copies, waits for them, and re-layouts, local(): lax.all_to_all(both_halves, 'row', split_axis=1, concat_axis=3, tiled=True)  67.5 us
    another operation x1, local copies, waits for them, and re-layouts, local(): both_halves = jnp.stack([lower_half, upper_half], axis=2)  62 us
    all_to_all x1, blocking collectives, local(): lax.all_to_all(spectral, 'col', split_axis=1, concat_axis=2, tiled=True)  52.2 us
    all_to_all x1, waiting for transfers between devices, local(): lax.all_to_all(mixed_in, 'col', split_axis=2, concat_axis=1, tiled=True)  48.3 us
    dot_general x1, matrix products, local(): jnp.dot(normed, gate_weight, preferred_element_type=jnp.float32)  26 us
  transfers between devices with their start and end apart: 2, of which 2 were waited for; matrix products, arithmetic and copies ran while one was open for 0% of the time, Pallas kernels for 0%

commit v1 on v0

v1 whole, which is shorter than its diff:
```python
import functools
import math

import jax
import jax.numpy as jnp
import numpy as np
from jax import lax
from jax.experimental import pallas as pl
from jax.experimental.pallas import tpu as pltpu
from jax.sharding import PartitionSpec as P

GROUP_DIM = 128
HALF = GROUP_DIM // 2
BF16 = jnp.bfloat16
F32 = jnp.float32
AXES = ("row", "col")


def angles(left, right, period):
    return (np.outer(left, right) % period) * (2.0 * math.pi / period)


def channel_table():
    phase = angles(np.arange(GROUP_DIM), np.arange(HALF), GROUP_DIM)
    table = np.stack([np.cos(phase), np.sin(phase)], axis=-1)
    table[:, 0, 1] = np.cos(math.pi * np.arange(GROUP_DIM))
    return table.reshape(GROUP_DIM, GROUP_DIM) * GROUP_DIM ** -0.5


def channel_order():
    order = np.zeros((HALF, 2), np.int64)
    order[:, 0] = np.arange(HALF)
    order[:, 1] = GROUP_DIM - np.arange(HALF)
    order[0, 1] = HALF
    pick = np.zeros((GROUP_DIM, GROUP_DIM))
    pick[np.arange(GROUP_DIM), order.reshape(-1)] = 1.0
    return pick


def position_tables(devices, length, first):
    second, fold = length // first, first // devices
    phase = angles(np.arange(first), np.arange(first), first)
    cosine, sine = np.cos(phase), np.sin(phase)
    zero = np.zeros_like(cosine)
    from_left = np.concatenate([cosine, sine, cosine, sine], axis=1)
    from_right = np.concatenate([-sine, cosine, sine, -cosine], axis=1)
    lone_left = np.concatenate([cosine, sine, zero, zero], axis=1)
    lone_right = np.concatenate([zero, zero, cosine, sine], axis=1)

    def interleave(left, right):
        pair = np.stack([left.reshape(devices, fold, -1), right.reshape(devices, fold, -1)], axis=1)
        return pair.reshape(2 * first, 4 * first)

    turn = angles(np.arange(second), np.arange(first), length)
    last = angles(np.arange(second), np.arange(second), second)
    closing = np.concatenate([np.cos(last), -np.sin(last)], axis=1) * length ** -0.5
    return (
        interleave(from_left, from_right),
        interleave(lone_left, lone_right),
        np.cos(turn),
        np.sin(turn),
        closing,
    )


def transform_kernel(first, direct, x_ref, g_ref, cos_ref, sin_ref, close_ref, out_ref):
    cosine, sine = cos_ref[...], sin_ref[...]
    seqs = x_ref.shape[2] if direct else x_ref.shape[1]
    for seq in range(seqs):
        if direct:
            x = x_ref[:, 0, seq].reshape(2 * first, x_ref.shape[-1])
        else:
            x = x_ref[0, seq]
        u = lax.dot_general(x, g_ref[0], (((0,), (0,)), ((), ())), preferred_element_type=F32)
        halves = []
        for half in range(2):
            real = u[:, 2 * half * first : (2 * half + 1) * first]
            imag = u[:, (2 * half + 1) * first : (2 * half + 2) * first]
            turned = jnp.concatenate(
                [(real * cosine - imag * sine).astype(BF16), (real * sine + imag * cosine).astype(BF16)], axis=0
            )
            halves.append(turned)
        turned = jnp.concatenate(halves, axis=1)
        y = jnp.dot(close_ref[...], turned, preferred_element_type=F32)
        if direct:
            out_ref[:, seq] = y.reshape(out_ref.shape[0], out_ref.shape[2], out_ref.shape[3]).astype(BF16)
        else:
            out_ref[seq] = y.astype(BF16)


def position_transform(x, lone_here, devices, length, first):
    _, pairs, seqs, rows, second = x.shape
    normal, lone, cosine, sine, closing = position_tables(devices, length, first)
    normal, lone = jnp.asarray(normal, BF16), jnp.asarray(lone, BF16)
    g = jnp.stack([jnp.where(lone_here, lone, normal), normal])
    direct = rows % 8 == 0 and second // devices >= 8
    if direct:
        x_spec = pl.BlockSpec((devices, 1, seqs, rows, second), lambda p: (0, p, 0, 0, 0))
        out_shape = (devices, seqs, second // devices, pairs * 2 * first)
        out_spec = pl.BlockSpec((devices, seqs, second // devices, 2 * first), lambda p: (0, 0, 0, p))
    else:
        x = x.transpose(1, 2, 0, 3, 4).reshape(pairs, seqs, devices * rows, second)
        x_spec = pl.BlockSpec((1, seqs, devices * rows, second), lambda p: (p, 0, 0, 0))
        out_shape = (seqs, second, pairs * 2 * first)
        out_spec = pl.BlockSpec((seqs, second, 2 * first), lambda p: (0, 0, p))
    whole = lambda p: (0, 0)
    y = pl.pallas_call(
        functools.partial(transform_kernel, first, direct),
        grid=(pairs,),
        in_specs=[
            x_spec,
            pl.BlockSpec((1, 2 * first, 4 * first), lambda p: (jnp.minimum(p, 1), 0, 0)),
            pl.BlockSpec((second, first), whole),
            pl.BlockSpec((second, first), whole),
            pl.BlockSpec((second, 2 * second), whole),
        ],
        out_specs=out_spec,
        out_shape=jax.ShapeDtypeStruct(out_shape, BF16),
        compiler_params=pltpu.CompilerParams(dimension_semantics=("arbitrary",)),
        cost_estimate=pl.CostEstimate(
            flops=pairs * seqs * second * first * 16 * (first + second), bytes_accessed=4 * x.size, transcendentals=0
        ),
    )(x, g, jnp.asarray(cosine, F32), jnp.asarray(sine, F32), jnp.asarray(closing, BF16))
    if direct:
        return y
    here = length // devices
    width = min(first, here)
    y = y.reshape(seqs, devices, here // width, -1, pairs * 2, width) if first <= here else (
        y.reshape(seqs, second, pairs * 2, first // here, here).transpose(0, 1, 3, 2, 4)
        .reshape(seqs, devices, 1, 1, pairs * 2, here)
    )
    return y.reshape(seqs, devices, here // width, -1).transpose(1, 0, 2, 3)


def local(devices, tokens, norm_gain, mix_weight, gate_weight, out_weight):
    seqs, here, width = tokens.shape
    length = here * devices
    mixed = mix_weight.shape[1]
    groups = mixed // GROUP_DIM
    pairs = mixed // devices // 2
    first = max(GROUP_DIM, devices)
    fold = first // devices
    second = length // first

    mix = jnp.einsum(
        "dgj,jk->dgk", mix_weight.reshape(width, groups, GROUP_DIM), jnp.asarray(channel_table(), BF16),
        preferred_element_type=F32,
    ).astype(BF16).reshape(width, mixed)
    widened = tokens.astype(F32)
    inverse_rms = lax.rsqrt(jnp.mean(widened * widened, axis=-1, keepdims=True) + 1e-06)
    normed = (widened * inverse_rms * norm_gain).astype(BF16)
    columns = lax.dot_general(
        mix, normed, (((0,), (2,)), ((), ())), preferred_element_type=F32
    ).astype(BF16)
    sent = columns.reshape(devices, pairs, 2, seqs, fold, second).transpose(0, 1, 3, 2, 4, 5)
    sent = sent.reshape(devices, pairs, seqs, 2 * fold, second)
    arrived = lax.all_to_all(sent, AXES, split_axis=0, concat_axis=0, tiled=True)

    gate_value = jax.nn.sigmoid(jnp.dot(normed, gate_weight, preferred_element_type=F32)).astype(BF16)
    ordered = jnp.einsum(
        "ij,gjd->gid", jnp.asarray(channel_order(), BF16), out_weight.reshape(groups, GROUP_DIM, width),
        preferred_element_type=F32,
    ).astype(BF16).reshape(mixed, width)
    gate_value, ordered, arrived = lax.optimization_barrier((gate_value, ordered, arrived))

    lone_here = lax.axis_index(AXES) * pairs % HALF == 0
    spectra = position_transform(arrived, lone_here, devices, length, first)
    returned = lax.all_to_all(spectra, AXES, split_axis=0, concat_axis=0, tiled=True)
    span = min(first, here)
    returned = returned.reshape(devices, seqs, here // span, 2 * pairs, span)
    spectral = returned.transpose(1, 2, 4, 0, 3).reshape(seqs, here, mixed)
    mapped = jnp.dot(spectral, ordered, preferred_element_type=F32)
    return (gate_value * mapped).astype(BF16)


def solution(mesh):
    in_specs = (P(None, AXES, None), P(), P(), P(), P())
    devices = mesh.shape["row"] * mesh.shape["col"]
    body = functools.partial(local, devices)
    return jax.shard_map(body, mesh=mesh, in_specs=in_specs, out_specs=P(None, AXES, None), check_vma=False)
```

time: 809 us -> 281 us (0.35); the launches traced: 794 us -> 280 us
  local copies, waits for them, and re-layouts: 312 us -> 31.6 us
  matrix products: 149 us -> 58.7 us
  waiting for transfers between devices: 141 us -> 61.5 us
  blocking collectives: 149 us -> 98.7 us
  other arithmetic: 29.8 us -> 6.15 us
  Pallas kernels: 0 us -> 15.8 us
    dot_general x11 -> x5, matrix products: 149 us -> 58.7 us  [the longest x1 26.3 us: local(): jnp.dot(normed, gate_weight, preferred_element_type=F32)]
    all_to_all x5 -> x0, local copies, waits for them, and re-layouts: 84.8 us -> none  [the longest x1 67.5 us: local(): lax.all_to_all(both_halves, 'row', split_axis=1, concat_axis=3, tiled=True)]
    all_to_all x2 -> x1, waiting for transfers between devices: 141 us -> 61.5 us  [local(): lax.all_to_all(sent, AXES, split_axis=0, concat_axis=0, tiled=True)]
    another operation x3 -> x0, local copies, waits for them, and re-layouts: 74.9 us -> none  [the longest x1 62 us: local(): both_halves = jnp.stack([lower_half, upper_half], axis=2)]
    unnamed x30 -> x18, local copies, waits for them, and re-layouts: 74.1 us -> 1.04 us
    all_to_all x2 -> x1, blocking collectives: 149 us -> 98.7 us  [local(): lax.all_to_all(spectra, AXES, split_axis=0, concat_axis=0, tiled=True)]
    another operation x3 -> x2, other arithmetic: 18.4 us -> 0.89 us  [position_transform(): g = jnp.stack([jnp.where(lone_here, lone, normal), normal])]
    pallas_call x0 -> x1, Pallas kernels: none -> 15.8 us  [position_transform(): pl.pallas_call(functools.partial(transform_kernel, first, direct), grid=(...]
  transfers between devices with their start and end apart: 2 -> 1, of which waited for: 2 -> 1; matrix products, arithmetic and copies ran while one was open for 0% -> 12% of each run, Pallas kernels for 0% -> 0%
where the time goes in v1:
time: 281 us; the launch traced here: 280 us
  blocking collectives  98.7 us (35%)
  waiting for transfers between devices  61.5 us (22%)
  matrix products  58.7 us (21%)
  local copies, waits for them, and re-layouts  31.6 us (11%)
  Pallas kernels  15.8 us (6%)
  starting transfers between devices  7.65 us (3%)
  other arithmetic  6.15 us (2%)
    all_to_all x1, blocking collectives, local(): lax.all_to_all(spectra, AXES, split_axis=0, concat_axis=0, tiled=True)  98.7 us
    all_to_all x1, waiting for transfers between devices, local(): lax.all_to_all(sent, AXES, split_axis=0, concat_axis=0, tiled=True)  61.5 us
    dot_general x1, matrix products, local(): jnp.dot(normed, gate_weight, preferred_element_type=F32)  26.3 us
    pallas_call x1, Pallas kernels, position_transform(): pl.pallas_call(functools.partial(transform_kernel, first, direct), grid=(...  15.8 us
    dot_general x1, matrix products, local(): mapped = jnp.dot(spectral, ordered, preferred_element_type=F32)  15.3 us
    reshape x2, local copies, waits for them, and re-layouts, local(): columns.reshape(devices, pairs, 2, seqs, fold, second)  14 us
    dot_general x1, matrix products, local(): lax.dot_general(mix, normed, (((0,), (2,)), ((), ())), preferred_element_...  10.5 us
    all_to_all x1, starting transfers between devices, local(): lax.all_to_all(sent, AXES, split_axis=0, concat_axis=0, tiled=True)  7.65 us
  transfers between devices with their start and end apart: 1, of which 1 were waited for; matrix products, arithmetic and copies ran while one was open for 12% of the time, Pallas kernels for 0%

profile of v1, /device:TPU:0, one launch (start us, length us, event | category | flops | bytes accessed | tf_op | source)
XLA Modules:
  0.0 280.2 jit_solution(10530616805701079769)
XLA Ops:
  0.0 0.0 copy-start.5
  0.0 0.0 slice-start
  0.0 0.0 copy-start
  0.0 0.0 copy-start.6
  0.0 5.2 %fusion = f32[2,1024]{1,0:T(2,128)S(1)} fusion(bf16[2,1024,2048]{2,1,0:T(8,128)(2,1)} %param.12), kind=kLoop, calls=%fused_computation.2 | loop fusion | flops 12580864 | bytes 8396800 | tf_op jit(solution)/shard_map/reduce_sum | solution.py:150
  5.3 0.0 copy-done.5
  5.3 0.0 copy-done
  5.3 0.0 slice-start.1
  5.3 1.3 fusion.14
  6.6 0.0 slice-done
  6.6 0.0 copy-done.6
  6.6 1.0 slice-done.1
  7.6 10.5 %fusion.17 = bf16[1024,2,1024]{2,0,1:T(8,128)(2,1)} fusion(bf16[2048,1024,1]{0,1,2:T(8,128)(2,1)S(1)} %bitcast.54, bf16[2,1024,2048]{2,1,0:T(8,128)(2,1)S(1)} %bitcast.51, f32[2048]{0:T(1024)S(1)} %copy-done.6, f32[2,1024]{1,0:T(2,128)S(1)} %add_rsqrt_fusion), kind=kOutput, calls=%fused_computation.18 | convolution fusion | flops 8608808960 | bytes 16793600 | tf_op jit(solution)/shard_map/dot_general | solution.py:152
  18.2 7.8 %reshape.37 = bf16[32,16,2,2,4,256]{5,4,2,1,0,3:T(4,128)(2,1)} reshape(bf16[1024,2,1024]{2,0,1:T(8,128)(2,1)} %fusion.17) | data formatting | bytes 8388608 | tf_op jit(solution)/shard_map/reshape | solution.py:155
  26.0 6.1 %copy.30 = bf16[32,16,2,2,4,256]{5,4,2,3,1,0:T(4,128)(2,1)} copy(bf16[32,16,2,2,4,256]{5,4,2,1,0,3:T(4,128)(2,1)} %reshape.37) | data formatting | bytes 8388608 | tf_op jit(solution)/shard_map/reshape | solution.py:155
  32.1 0.0 copy-start.2
  32.1 0.0 copy-start.3
  32.1 7.0 %reshape.38 = bf16[32,16,2,8,256]{4,3,2,1,0:T(8,128)(2,1)} reshape(bf16[32,16,2,2,4,256]{5,4,3,2,1,0:T(4,128)(2,1)} %bitcast.49) | data formatting | bytes 8388608 | tf_op jit(solution)/shard_map/reshape | solution.py:156
  39.1 7.6 %all-to-all-start = ((bf16[32,16,2,8,256]{4,3,2,1,0:T(8,128)(2,1)}), bf16[32,16,2,8,256]{4,3,2,1,0:T(8,128)(2,1)}, u32[]{:S(2)}, u32[]{:S(2)}) async-start(bf16[32,16,2,8,256]{4,3,2,1,0:T(8,128)(2,1)} %reshape.38), calls=%async_computation | async-start | bytes 8388608 | tf_op jit(solution)/shard_map/all_to_all | solution.py:157
  46.8 0.0 copy-done.2
  46.8 0.0 copy-done.3
  46.9 0.0 copy-done.1
  46.9 0.9 pad_maximum_fusion.g_ref
  47.7 0.0 copy-done.4
  47.7 5.4 %convolution_convert_fusion = bf16[128,8,2048]{2,0,1:T(8,128)(2,1)} fusion(bf16[128,128,1]{1,0,2:T(8,128)(2,1)S(1)} %copy-done.4, bf16[8,128,2048]{2,1,0:T(8,128)(2,1)} %bitcast.52), kind=kOutput, calls=%fused_computation.17 | convolution fusion | flops 538968064 | bytes 8421376 | tf_op jit(solution)/shard_map/ij,gjd->gid/dot_general | solution.py:160
  53.1 26.3 %divide_convert_fusion = bf16[2,1024,2048]{2,1,0:T(8,128)(2,1)} fusion(bf16[2048,2048]{1,0:T(8,128)(2,1)} %param.15, bf16[2,1024,2048]{2,1,0:T(8,128)(2,1)} %param.12, f32[2048]{0:T(1024)S(1)} %copy-done.6, f32[2,1024]{1,0:T(2,128)S(1)} %add_rsqrt_fusion), kind=kOutput, calls=%fused_computation.6 | convolution fusion | flops 17213423616 | bytes 25182208 | tf_op jit(solution)/shard_map/dot_general | solution.py:159
  79.4 61.5 %all-to-all-done.x_ref = bf16[32,16,2,8,256]{4,3,2,1,0:T(8,128)(2,1)} async-done(((bf16[32,16,2,8,256]{4,3,2,1,0:T(8,128)(2,1)}), bf16[32,16,2,8,256]{4,3,2,1,0:T(8,128)(2,1)}, u32[]{:S(2)}, u32[]{:S(2)}) %all-to-all-start) | async-done | bytes 4194336 | tf_op jit(solution)/shard_map/all_to_all | solution.py:157
  140.9 15.8 %shard_map.118 = bf16[32,2,8,4096]{3,2,1,0:T(8,128)(2,1)} custom-call(bf16[32,16,2,8,256]{4,3,2,1,0:T(8,128)(2,1)} %all-to-all-done.x_ref, bf16[2,256,512]{2,1,0:T(8,128)(2,1)} %pad_maximum_fusion.g_ref, f32[256,128]{1,0:T(8,128)} %constant.54.clone.cos_ref, f32[256,128]{1,0:T(8,128)} %constant.55.clone.sin_ref, bf16[256,512]{1,0:T(8,128)(2,1)} %constant.56.clone.close_ref), custom_call_target="tpu_custom_call" | custom-call | flops 6442450944 | bytes 8388608 | tf_op jit(solution)/shard_map/pallas_call | solution.py:107
  156.7 98.7 %all_to_all.10 = bf16[32,2,8,4096]{3,2,1,0:T(8,128)(2,1)S(1)} all-to-all(bf16[32,2,8,4096]{3,2,1,0:T(8,128)(2,1)} %shard_map.118), channel_id=1, replica_groups=mesh['row'=8,'col'=4] {'row','col'}, dimensions={0} | all-to-all | bytes 8388608 | tf_op jit(solution)/shard_map/all_to_all | solution.py:168
  255.4 2.2 copy_bitcast_fusion
  257.6 7.4 %reshape.40 = bf16[2,1024,1024]{1,2,0:T(8,128)(2,1)} reshape(bf16[2,8,128,32,32]{2,1,4,3,0:T(8,128)(2,1)} %copy_bitcast_fusion) | data formatting | bytes 8388608 | tf_op jit(solution)/shard_map/reshape | solution.py:171
  265.0 15.3 %multiply_convert_fusion = bf16[2,1024,2048]{2,1,0:T(8,128)(2,1)} fusion(bf16[2,1024,2048]{2,1,0:T(8,128)(2,1)} %divide_convert_fusion, bf16[2,1024,1024]{1,2,0:T(8,128)(2,1)} %reshape.40, bf16[1024,2048]{1,0:T(8,128)(2,1)} %bitcast.53), kind=kOutput, calls=%fused_computation.5 | convolution fusion | flops 8602517504 | bytes 25165824 | tf_op jit(solution)/shard_map/dot_general | solution.py:172
  (5 shorter events, 0.0 us)
Async XLA Ops:
  0.0 5.3 %copy-start.5 = (bf16[128,128,1]{0,1,2:T(8,128)(2,1)S(1)}, bf16[128,128,1]{0,1,2:T(8,128)(2,1)}, u32[]{:S(2)}) copy-start(bf16[128,128,1]{0,1,2:T(8,128)(2,1)} %constant.59) | copy-start | bytes 98308
  0.0 6.6 %slice-start = ((s8[8388608]{0:T(1024)(128)(4,1)}), s8[4194304]{0:T(1024)(128)(4,1)S(1)}, s32[]{:S(2)}) async-start(s8[8388608]{0:T(1024)(128)(4,1)} %bitcast.50), calls=%async_computation.2 | async-start | bytes 8388608
  0.0 5.3 %copy-start = (bf16[2048,1024]{1,0:T(8,128)(2,1)S(1)}, bf16[2048,1024]{1,0:T(8,128)(2,1)}, u32[]{:S(2)}) copy-start(bf16[2048,1024]{1,0:T(8,128)(2,1)} %param.14) | copy-start | bytes 12582916
  0.0 6.6 %copy-start.6 = (f32[2048]{0:T(1024)S(1)}, f32[2048]{0:T(1024)}, u32[]{:S(2)}) copy-start(f32[2048]{0:T(1024)} %param.13) | copy-start | bytes 24580
  5.3 2.3 slice-start.1
  32.1 14.7 %copy-start.2 = (bf16[256,512]{1,0:T(8,128)(2,1)S(1)}, bf16[256,512]{1,0:T(8,128)(2,1)}, u32[]{:S(2)}) copy-start(bf16[256,512]{1,0:T(8,128)(2,1)} %constant.53.clone) | copy-start | bytes 786436
  32.1 14.7 %copy-start.3 = (bf16[256,512]{1,0:T(8,128)(2,1)S(1)}, bf16[256,512]{1,0:T(8,128)(2,1)}, u32[]{:S(2)}) copy-start(bf16[256,512]{1,0:T(8,128)(2,1)} %constant.52.clone) | copy-start | bytes 786436
  32.1 14.7 %copy-start.1 = (bf16[1,256,512]{2,1,0:T(8,128)(2,1)S(1)}, bf16[1,256,512]{2,1,0:T(8,128)(2,1)}, u32[]{:S(2)}) copy-start(bf16[1,256,512]{2,1,0:T(8,128)(2,1)} %constant.57) | copy-start | bytes 786436
  32.1 15.6 %copy-start.4 = (bf16[128,128,1]{1,0,2:T(8,128)(2,1)S(1)}, bf16[128,128,1]{1,0,2:T(8,128)(2,1)}, u32[]{:S(2)}) copy-start(bf16[128,128,1]{1,0,2:T(8,128)(2,1)} %constant.58) | copy-start | bytes 98308
  39.1 101.7 %all-to-all-start = ((bf16[32,16,2,8,256]{4,3,2,1,0:T(8,128)(2,1)}), bf16[32,16,2,8,256]{4,3,2,1,0:T(8,128)(2,1)}, u32[]{:S(2)}, u32[]{:S(2)}) async-start(bf16[32,16,2,8,256]{4,3,2,1,0:T(8,128)(2,1)} %reshape.38), calls=%async_computation | async-start | bytes 8388608 | tf_op jit(solution)/shard_map/all_to_all | solution.py:157

commit v2 on v1

v2 whole, which is shorter than its diff:
```python
import functools
import math

import jax
import jax.numpy as jnp
import numpy as np
from jax import lax
from jax.experimental import pallas as pl
from jax.experimental.pallas import tpu as pltpu
from jax.sharding import PartitionSpec as P

GROUP_DIM = 128
HALF = GROUP_DIM // 2
BF16 = jnp.bfloat16
F32 = jnp.float32
AXES = ("row", "col")
LANES = 128
STEP = 8


def angles(left, right, period):
    return (np.outer(left, right) % period) * (2.0 * math.pi / period)


def channel_table():
    phase = angles(np.arange(GROUP_DIM), np.arange(HALF), GROUP_DIM)
    table = np.stack([np.cos(phase), np.sin(phase)], axis=-1)
    table[:, 0, 1] = np.cos(math.pi * np.arange(GROUP_DIM))
    return table.reshape(GROUP_DIM, GROUP_DIM) * GROUP_DIM ** -0.5


def channel_order():
    order = np.zeros((HALF, 2), np.int64)
    order[:, 0] = np.arange(HALF)
    order[:, 1] = GROUP_DIM - np.arange(HALF)
    order[0, 1] = HALF
    pick = np.zeros((GROUP_DIM, GROUP_DIM))
    pick[np.arange(GROUP_DIM), order.reshape(-1)] = 1.0
    return pick


def position_tables(devices, length, first):
    second, fold = length // first, first // devices
    phase = angles(np.arange(first), np.arange(first), first)
    cosine, sine = np.cos(phase), np.sin(phase)
    zero = np.zeros_like(cosine)
    from_left = np.concatenate([cosine, sine, cosine, sine], axis=1)
    from_right = np.concatenate([-sine, cosine, sine, -cosine], axis=1)
    lone_left = np.concatenate([cosine, sine, zero, zero], axis=1)
    lone_right = np.concatenate([zero, zero, cosine, sine], axis=1)

    def interleave(left, right):
        pair = np.stack([left, right]).reshape(2, devices, fold, -1).transpose(0, 2, 1, 3)
        return pair.reshape(2 * first, 4 * first)

    turn = angles(np.arange(second), np.arange(first), length)
    last = angles(np.arange(second), np.arange(second), second)
    closing = np.concatenate([np.cos(last), -np.sin(last)], axis=1) * length ** -0.5
    return (
        interleave(from_left, from_right),
        interleave(lone_left, lone_right),
        np.cos(turn),
        np.sin(turn),
        closing,
    )


def turn_halves(u, cosine, sine, first):
    halves = []
    for half in range(2):
        real = u[..., 2 * half * first : (2 * half + 1) * first]
        imag = u[..., (2 * half + 1) * first : (2 * half + 2) * first]
        halves.append(
            jnp.concatenate(
                [(real * cosine - imag * sine).astype(BF16), (real * sine + imag * cosine).astype(BF16)], axis=-2
            )
        )
    return jnp.concatenate(halves, axis=-1)


def transform_kernel(first, x_ref, g_ref, cos_ref, sin_ref, close_ref, out_ref, rows_in, rows_out):
    devices, channels, here = x_ref.shape
    second = cos_ref.shape[0]
    fold, tiles = here // second, second // LANES
    for tile in range(here // LANES):
        rows_in[tile] = (
            x_ref[:, :, tile * LANES : (tile + 1) * LANES].astype(F32).reshape(devices * channels, LANES)
        )
    cosine, sine = cos_ref[...], sin_ref[...]
    for pair in range(channels // 2):
        rows = []
        for column in range(2):
            for high in range(fold):
                picked = pl.ds(2 * pair + column, devices, stride=channels)
                rows.append(
                    jnp.concatenate(
                        [rows_in[high * tiles + tile, picked, :] for tile in range(tiles)], axis=1
                    ).astype(BF16)
                )
        x = jnp.concatenate(rows, axis=0)
        g = g_ref[0] if pair == 0 else g_ref[1]
        if pair == 0:
            g = jnp.where(pl.program_id(0) == 0, g, g_ref[1])
        u = lax.dot_general(x, g, (((0,), (0,)), ((), ())), preferred_element_type=F32)
        turned = turn_halves(u, cosine, sine, first)
        y = jnp.dot(close_ref[...], turned, preferred_element_type=F32)
        for half in range(2):
            rows_out[pl.ds(2 * pair + half, second, stride=channels), :] = y[:, half * first : (half + 1) * first]
    out_ref[...] = rows_out[...].reshape(out_ref.shape).astype(BF16)


def position_transform(x, lone_here, devices, length, first):
    _, channels, here = x.shape
    second, fold = length // first, first // devices
    normal, lone, cosine, sine, closing = position_tables(devices, length, first)
    normal, lone = jnp.asarray(normal, BF16), jnp.asarray(lone, BF16)
    cosine, sine, closing = jnp.asarray(cosine, F32), jnp.asarray(sine, F32), jnp.asarray(closing, BF16)
    g = jnp.stack([jnp.where(lone_here, lone, normal), normal])
    if not fits(channels, here, first, devices):
        pairs, span = channels // 2, min(first, here)
        x = x.reshape(devices, pairs, 2, fold, second).transpose(1, 2, 3, 0, 4).reshape(pairs, 2 * first, second)
        g = jnp.stack([g[min(pair, 1)] for pair in range(pairs)])
        u = jnp.einsum("pxr,pxj->prj", x, g, preferred_element_type=F32)
        y = jnp.einsum("kx,pxj->pkj", closing, turn_halves(u, cosine, sine, first), preferred_element_type=F32)
        y = y.astype(BF16).reshape(pairs, second, 2, first).transpose(1, 3, 0, 2)
        return y.reshape(devices, here // span, span, channels).transpose(0, 1, 3, 2)
    low = second // devices
    whole = lambda step: (0, 0)
    return pl.pallas_call(
        functools.partial(transform_kernel, first),
        grid=(channels // STEP,),
        in_specs=[
            pl.BlockSpec((devices, STEP, here), lambda step: (0, step, 0)),
            pl.BlockSpec((2, 2 * first, 4 * first), lambda step: (0, 0, 0)),
            pl.BlockSpec((second, first), whole),
            pl.BlockSpec((second, first), whole),
            pl.BlockSpec((second, 2 * second), whole),
        ],
        out_specs=pl.BlockSpec((devices, low, STEP, first), lambda step: (0, 0, step, 0)),
        out_shape=jax.ShapeDtypeStruct((devices, low, channels, first), BF16),
        scratch_shapes=[
            pltpu.VMEM((here // LANES, devices * STEP, LANES), F32),
            pltpu.VMEM((second * STEP, first), F32),
        ],
        compiler_params=pltpu.CompilerParams(dimension_semantics=("arbitrary",)),
        cost_estimate=pl.CostEstimate(
            flops=channels * second * first * 8 * (first + second), bytes_accessed=4 * x.size, transcendentals=0
        ),
    )(x, g, cosine, sine, closing)


def fits(channels, here, first, devices):
    return first == LANES and channels % STEP == 0 and devices % 16 == 0 and here % (2 * first) == 0


def closing_kernel(r_ref, w_ref, gate_ref, *rest):
    out_ref = rest[-1]
    mixed = w_ref.shape[0]
    span = r_ref.shape[3]
    left = jnp.concatenate([r_ref[:, low].reshape(mixed, span) for low in range(r_ref.shape[1])], axis=1)
    mapped = lax.dot_general(left, w_ref[...], (((0,), (0,)), ((), ())), preferred_element_type=F32)
    out_ref[0] = (gate_ref[0].astype(F32) * mapped).astype(BF16)


def close(seq, returned, ordered, gate_value, so_far):
    devices, lows, channels, span = returned.shape
    seqs, here, width = gate_value.shape
    mixed = ordered.shape[0]
    many = 2
    block = pl.BlockSpec((1, many * span, width), lambda step: (seq, step, 0))
    operands = [returned, ordered, gate_value]
    in_specs = [
        pl.BlockSpec((devices, many, channels, span), lambda step: (0, step, 0, 0)),
        pl.BlockSpec((mixed, width), lambda step: (0, 0)),
        block,
    ]
    if so_far is not None:
        operands.append(so_far)
        in_specs.append(pl.BlockSpec(memory_space=pl.ANY))
    return pl.pallas_call(
        closing_kernel,
        grid=(lows // many,),
        in_specs=in_specs,
        out_specs=block,
        out_shape=jax.ShapeDtypeStruct((seqs, here, width), BF16),
        input_output_aliases={} if so_far is None else {3: 0},
        compiler_params=pltpu.CompilerParams(dimension_semantics=("arbitrary",)),
        cost_estimate=pl.CostEstimate(
            flops=2 * here * mixed * width, bytes_accessed=2 * (here * mixed + mixed * width + 2 * here * width),
            transcendentals=0,
        ),
    )(*operands)


def local(devices, tokens, norm_gain, mix_weight, gate_weight, out_weight):
    seqs, here, width = tokens.shape
    length = here * devices
    mixed = mix_weight.shape[1]
    groups = mixed // GROUP_DIM
    channels = mixed // devices
    first = max(GROUP_DIM, devices)
    span = min(first, here)

    mix = jnp.einsum(
        "dgj,jk->dgk", mix_weight.reshape(width, groups, GROUP_DIM), jnp.asarray(channel_table(), BF16),
        preferred_element_type=F32,
    ).astype(BF16).reshape(width, mixed)

    def norm(x):
        widened = x.astype(F32)
        inverse_rms = lax.rsqrt(jnp.mean(widened * widened, axis=-1, keepdims=True) + 1e-06)
        return (widened * inverse_rms * norm_gain).astype(BF16)

    def exchange(x):
        return lax.all_to_all(x, AXES, split_axis=0, concat_axis=0, tiled=True)

    lone_here = lax.axis_index(AXES) * (channels // 2) % HALF == 0
    transform = functools.partial(
        position_transform, lone_here=lone_here, devices=devices, length=length, first=first
    )
    arrived = []
    for seq in range(seqs):
        columns = lax.dot_general(
            mix, norm(tokens[seq]), (((0,), (1,)), ((), ())), preferred_element_type=F32
        ).astype(BF16).reshape(devices, channels, here)
        if seq:
            columns, arrived[-1] = lax.optimization_barrier((columns, arrived[-1]))
        arrived.append(exchange(columns))

    gate_value = jax.nn.sigmoid(jnp.dot(norm(tokens), gate_weight, preferred_element_type=F32)).astype(BF16)
    ordered = jnp.einsum(
        "ij,gjd->gid", jnp.asarray(channel_order(), BF16), out_weight.reshape(groups, GROUP_DIM, width),
        preferred_element_type=F32,
    ).astype(BF16).reshape(mixed, width)
    gate_value, ordered, arrived[-1] = lax.optimization_barrier((gate_value, ordered, arrived[-1]))

    returned = []
    for seq in range(seqs):
        spectra = transform(arrived[seq])
        if seq:
            spectra, returned[-1] = lax.optimization_barrier((spectra, returned[-1]))
        returned.append(exchange(spectra))

    if fits(channels, here, first, devices):
        gated = None
        for seq in range(seqs):
            gated = close(seq, returned[seq], ordered, gate_value, gated)
        return gated
    spectral = jnp.stack(returned).transpose(0, 2, 4, 1, 3).reshape(seqs, here, mixed)
    mapped = jnp.dot(spectral, ordered, preferred_element_type=F32)
    return (gate_value * mapped).astype(BF16)


def solution(mesh):
    in_specs = (P(None, AXES, None), P(), P(), P(), P())
    devices = mesh.shape["row"] * mesh.shape["col"]
    body = functools.partial(local, devices)
    return jax.shard_map(body, mesh=mesh, in_specs=in_specs, out_specs=P(None, AXES, None), check_vma=False)
```

time: 281 us -> 241 us (0.86)
  blocking collectives: 98.7 us -> 0 us
  waiting for transfers between devices: 61.5 us -> 126 us
  local copies, waits for them, and re-layouts: 31.6 us -> 4.42 us
  Pallas kernels: 15.8 us -> 32.5 us
  matrix products: 58.7 us -> 46.5 us
  starting transfers between devices: 7.65 us -> 19.7 us
  other arithmetic: 6.15 us -> 11 us
    all_to_all x1 -> x0, blocking collectives: 98.7 us -> none  [local(): lax.all_to_all(spectra, AXES, split_axis=0, concat_axis=0, tiled=True)]
    all_to_all x1 -> x4, waiting for transfers between devices: 61.5 us -> 126 us  [exchange(): return lax.all_to_all(x, AXES, split_axis=0, concat_axis=0, tiled=True)]
    reshape x4 -> x0, local copies, waits for them, and re-layouts: 28.3 us -> none  [the longest x2 14 us: local(): columns.reshape(devices, pairs, 2, seqs, fold, second)]
    pallas_call x1 -> x4, Pallas kernels: 15.8 us -> 32.5 us  [the longest x2 18.9 us: close(): pl.pallas_call(closing_kernel, grid=(lows // many,), in_specs=in_specs, o...]
    all_to_all x1 -> x4, starting transfers between devices: 7.65 us -> 19.7 us  [exchange(): return lax.all_to_all(x, AXES, split_axis=0, concat_axis=0, tiled=True)]
    dot_general x3, matrix products: 52 us -> 41.9 us  [the longest x1 26.3 us: local(): jnp.dot(norm(tokens), gate_weight, preferred_element_type=F32)]
    reduce_sum x1 -> x2, other arithmetic: 5.25 us -> 10.1 us  [norm(): jnp.mean(widened * widened, axis=-1, keepdims=True) + 1e-06]
    unnamed x18 -> x28, local copies, waits for them, and re-layouts: 1.04 us -> 4.42 us
  transfers between devices with their start and end apart: 1 -> 4, of which waited for: 1 -> 4; matrix products, arithmetic and copies ran while one was open for 12% -> 19% of each run, Pallas kernels for 0% -> 10%
where the time goes in v2:
time: 241 us; the launch traced here: 240 us
  waiting for transfers between devices  126 us (52%)
  matrix products  46.5 us (19%)
  Pallas kernels  32.5 us (13%)
  starting transfers between devices  19.7 us (8%)
  other arithmetic  11 us (5%)
  local copies, waits for them, and re-layouts  4.42 us (2%)
    all_to_all x4, waiting for transfers between devices, exchange(): return lax.all_to_all(x, AXES, split_axis=0, concat_axis=0, tiled=True)  126 us
    dot_general x1, matrix products, local(): jnp.dot(norm(tokens), gate_weight, preferred_element_type=F32)  26.3 us
    all_to_all x4, starting transfers between devices, exchange(): return lax.all_to_all(x, AXES, split_axis=0, concat_axis=0, tiled=True)  19.7 us
    pallas_call x2, Pallas kernels, close(): pl.pallas_call(closing_kernel, grid=(lows // many,), in_specs=in_specs, o...  18.9 us
    dot_general x2, matrix products, local(): lax.dot_general(mix, norm(tokens[seq]), (((0,), (1,)), ((), ())), preferr...  15.7 us
    pallas_call x2, Pallas kernels, position_transform(): pl.pallas_call(functools.partial(transform_kernel, first), grid=(channels...  13.7 us
    reduce_sum x2, other arithmetic, norm(): jnp.mean(widened * widened, axis=-1, keepdims=True) + 1e-06  10.1 us
  transfers between devices with their start and end apart: 4, of which 4 were waited for; matrix products, arithmetic and copies ran while one was open for 19% of the time, Pallas kernels for 10%

profile of v2, /device:TPU:0, one launch (start us, length us, event | category | flops | bytes accessed | tf_op | source)
XLA Modules:
  0.0 240.3 jit_solution(2586095227350989311)
XLA Ops:
  0.0 4.5 %fusion.6 = (f32[1024]{0:T(1024)S(1)}, f32[1024]{0:T(1024)S(1)}) fusion(bf16[2,1024,2048]{2,1,0:T(8,128)(2,1)} %param.17), kind=kLoop, calls=%fused_computation.13 | loop fusion | flops 12580864 | bytes 8396800 | tf_op jit(solution)/shard_map/reduce_sum | solution.py:211
  4.5 0.0 copy-done.10
  4.5 0.3 copy-done.1
  4.8 1.3 fusion.31
  6.1 0.0 copy-start.3
  6.2 1.5 slice-done.1
  7.6 6.2 %fusion.39 = bf16[1024,1024]{1,0:T(8,128)(2,1)} fusion(bf16[2048,1024]{0,1:T(8,128)(2,1)S(1)} %bitcast.47, f32[1024]{0:T(1024)S(1)} %get-tuple-element.21, f32[2048]{0:T(1024)S(1)} %copy-done.11, bf16[2,1024,2048]{2,1,0:T(8,128)(2,1)S(1)} %bitcast.45), kind=kOutput, calls=%fused_computation.36 | convolution fusion | flops 4304404480 | bytes 10498048 | tf_op jit(solution)/shard_map/dot_general | solution.py:223
  13.8 7.3 %all-to-all-start = ((bf16[32,32,1024]{2,1,0:T(8,128)(2,1)}), bf16[32,32,1024]{2,1,0:T(8,128)(2,1)S(1)}, u32[]{:S(2)}, u32[]{:S(2)}) async-start(bf16[32,32,1024]{2,1,0:T(8,128)(2,1)} %bitcast.50), calls=%async_computation | async-start | bytes 4194304 | tf_op jit(solution)/shard_map/all_to_all | solution.py:215
  21.2 0.0 copy-start.7
  21.2 0.0 copy-start.8
  21.2 0.0 copy-start.6
  21.2 9.5 %fusion.36 = bf16[1024,1024]{1,0:T(8,128)(2,1)} fusion(bf16[2048,1024]{0,1:T(8,128)(2,1)} %bitcast.48, f32[2048]{0:T(1024)S(1)} %copy-done.11, f32[1024]{0:T(1024)S(1)} %get-tuple-element.22, bf16[2,1024,2048]{2,1,0:T(8,128)(2,1)} %param.17), kind=kOutput, calls=%fused_computation.35 | convolution fusion | flops 4304404480 | bytes 10498048 | tf_op jit(solution)/shard_map/dot_general | solution.py:223
  30.7 39.2 %all-to-all-done.x_ref = bf16[32,32,1024]{2,1,0:T(8,128)(2,1)S(1)} async-done(((bf16[32,32,1024]{2,1,0:T(8,128)(2,1)}), bf16[32,32,1024]{2,1,0:T(8,128)(2,1)S(1)}, u32[]{:S(2)}, u32[]{:S(2)}) %all-to-all-start) | async-done | bytes 2097184 | tf_op jit(solution)/shard_map/all_to_all | solution.py:215
  69.9 1.3 copy-done.5
  71.2 4.2 %all-to-all-start.1 = ((bf16[32,32,1024]{2,1,0:T(8,128)(2,1)}), bf16[32,32,1024]{2,1,0:T(8,128)(2,1)S(1)}, u32[]{:S(2)}, u32[]{:S(2)}) async-start(bf16[32,32,1024]{2,1,0:T(8,128)(2,1)} %bitcast.49), calls=%async_computation.1 | async-start | bytes 4194304 | tf_op jit(solution)/shard_map/all_to_all | solution.py:215
  75.4 0.0 copy-start.2
  75.5 0.8 pad_maximum_fusion.g_ref
  76.3 5.6 %fusion = f32[2,1024]{1,0:T(2,128)S(1)} fusion(bf16[2,1024,2048]{2,1,0:T(8,128)(2,1)} %param.17), kind=kLoop, calls=%fused_computation.2 | loop fusion | flops 12580864 | bytes 8396800 | tf_op jit(solution)/shard_map/reduce_sum | solution.py:211
  82.0 0.0 copy-done.9
  82.0 0.0 copy-done.2
  82.0 3.2 %convolution_convert_fusion = bf16[128,8,2048]{2,0,1:T(8,128)(2,1)} fusion(bf16[128,128,1]{1,0,2:T(8,128)(2,1)S(1)} %copy-done.9, bf16[8,128,2048]{2,1,0:T(8,128)(2,1)S(1)} %bitcast.46), kind=kOutput, calls=%fused_computation.32 | convolution fusion | flops 538968064 | bytes 8421376 | tf_op jit(solution)/shard_map/ij,gjd->gid/dot_general | solution.py:231
  85.2 6.8 %shard_map.164 = bf16[32,8,32,128]{3,2,1,0:T(8,128)(2,1)} custom-call(bf16[32,32,1024]{2,1,0:T(8,128)(2,1)} %copy-done.5, bf16[2,256,512]{2,1,0:T(8,128)(2,1)} %pad_maximum_fusion.g_ref, f32[256,128]{1,0:T(8,128)} %constant.58.clone.cos_ref, f32[256,128]{1,0:T(8,128)} %constant.59.clone.sin_ref, bf16[256,512]{1,0:T(8,128)(2,1)} %constant.60.clone.close_ref), custom_call_target="tpu_custom_call" | custom-call | flops 3221225472 | bytes 4194304 | tf_op jit(solution)/shard_map/pallas_call | solution.py:129
  92.1 31.9 %all-to-all-done.1.x_ref = bf16[32,32,1024]{2,1,0:T(8,128)(2,1)S(1)} async-done(((bf16[32,32,1024]{2,1,0:T(8,128)(2,1)}), bf16[32,32,1024]{2,1,0:T(8,128)(2,1)S(1)}, u32[]{:S(2)}, u32[]{:S(2)}) %all-to-all-start.1) | async-done | bytes 2097184 | tf_op jit(solution)/shard_map/all_to_all | solution.py:215
  123.9 1.3 copy-done.4
  125.3 4.0 %all-to-all-start.2 = ((bf16[32,8,32,128]{3,2,1,0:T(8,128)(2,1)}), bf16[32,8,32,128]{3,2,1,0:T(8,128)(2,1)S(1)}, u32[]{:S(2)}, u32[]{:S(2)}) async-start(bf16[32,8,32,128]{3,2,1,0:T(8,128)(2,1)} %shard_map.164), calls=%async_computation.2 | async-start | bytes 4194304 | tf_op jit(solution)/shard_map/all_to_all | solution.py:215
  129.3 26.3 %divide_convert_fusion.gate_ref = bf16[2,1024,2048]{2,1,0:T(8,128)(2,1)} fusion(bf16[2048,2048]{1,0:T(8,128)(2,1)} %param.20, bf16[2,1024,2048]{2,1,0:T(8,128)(2,1)} %param.17, f32[2048]{0:T(1024)S(1)} %copy-done.11, f32[2,1024]{1,0:T(2,128)S(1)} %add_rsqrt_fusion), kind=kOutput, calls=%fused_computation.5 | convolution fusion | flops 17213423616 | bytes 25182208 | tf_op jit(solution)/shard_map/dot_general | solution.py:230
  155.5 6.8 %shard_map.163 = bf16[32,8,32,128]{3,2,1,0:T(8,128)(2,1)} custom-call(bf16[32,32,1024]{2,1,0:T(8,128)(2,1)} %copy-done.4, bf16[2,256,512]{2,1,0:T(8,128)(2,1)} %pad_maximum_fusion.g_ref, f32[256,128]{1,0:T(8,128)} %constant.58.clone.cos_ref, f32[256,128]{1,0:T(8,128)} %constant.59.clone.sin_ref, bf16[256,512]{1,0:T(8,128)(2,1)} %constant.60.clone.close_ref), custom_call_target="tpu_custom_call" | custom-call | flops 3221225472 | bytes 4194304 | tf_op jit(solution)/shard_map/pallas_call | solution.py:129
  162.4 15.6 %all-to-all-done.2.r_ref = bf16[32,8,32,128]{3,2,1,0:T(8,128)(2,1)S(1)} async-done(((bf16[32,8,32,128]{3,2,1,0:T(8,128)(2,1)}), bf16[32,8,32,128]{3,2,1,0:T(8,128)(2,1)S(1)}, u32[]{:S(2)}, u32[]{:S(2)}) %all-to-all-start.2) | async-done | bytes 2097184 | tf_op jit(solution)/shard_map/all_to_all | solution.py:215
  178.0 4.1 %all-to-all-start.3 = ((bf16[32,8,32,128]{3,2,1,0:T(8,128)(2,1)}), bf16[32,8,32,128]{3,2,1,0:T(8,128)(2,1)}, u32[]{:S(2)}, u32[]{:S(2)}) async-start(bf16[32,8,32,128]{3,2,1,0:T(8,128)(2,1)} %shard_map.163), calls=%async_computation.3 | async-start | bytes 4194304 | tf_op jit(solution)/shard_map/all_to_all | solution.py:215
  182.2 9.4 %shard_map.165.rest_0_ = bf16[2,1024,2048]{2,1,0:T(8,128)(2,1)} custom-call(bf16[32,8,32,128]{3,2,1,0:T(8,128)(2,1)} %copy-done, bf16[1024,2048]{1,0:T(8,128)(2,1)} %bitcast.42, bf16[2,1024,2048]{2,1,0:T(8,128)(2,1)} %divide_convert_fusion.gate_ref), custom_call_target="tpu_custom_call" | custom-call | flops 4294967296 | bytes 14680064 | tf_op jit(solution)/shard_map/pallas_call | solution.py:180
  191.6 39.2 %all-to-all-done.3.r_ref = bf16[32,8,32,128]{3,2,1,0:T(8,128)(2,1)} async-done(((bf16[32,8,32,128]{3,2,1,0:T(8,128)(2,1)}), bf16[32,8,32,128]{3,2,1,0:T(8,128)(2,1)}, u32[]{:S(2)}, u32[]{:S(2)}) %all-to-all-start.3) | async-done | bytes 2097184 | tf_op jit(solution)/shard_map/all_to_all | solution.py:215
  230.8 9.4 %shard_map.166 = bf16[2,1024,2048]{2,1,0:T(8,128)(2,1)} custom-call(bf16[32,8,32,128]{3,2,1,0:T(8,128)(2,1)} %all-to-all-done.3.r_ref, bf16[1024,2048]{1,0:T(8,128)(2,1)} %bitcast.43, bf16[2,1024,2048]{2,1,0:T(8,128)(2,1)} %divide_convert_fusion.gate_ref, bf16[2,1024,2048]{2,1,0:T(8,128)(2,1)} %shard_map.165.rest_0_), custom_call_target="tpu_custom_call", output_to_operand_aliasing={{}: (3, {})} | custom-call | flops 4294967296 | bytes 14680064 | tf_op jit(solution)/shard_map/pallas_call | solution.py:180
  (20 shorter events, 0.1 us)
Async XLA Ops:
  0.0 4.5 %copy-start.10 = (bf16[128,128,1]{0,1,2:T(8,128)(2,1)S(1)}, bf16[128,128,1]{0,1,2:T(8,128)(2,1)}, u32[]{:S(2)}) copy-start(bf16[128,128,1]{0,1,2:T(8,128)(2,1)} %constant.63) | copy-start | bytes 98308
  0.0 6.1 %slice-start = ((s8[8388608]{0:T(1024)(128)(4,1)}), s8[4194304]{0:T(1024)(128)(4,1)S(1)}, s32[]{:S(2)}) async-start(s8[8388608]{0:T(1024)(128)(4,1)} %bitcast.44), calls=%async_computation.4 | async-start | bytes 8388608
  0.0 4.8 %copy-start.1 = (bf16[2048,1024]{1,0:T(8,128)(2,1)S(1)}, bf16[2048,1024]{1,0:T(8,128)(2,1)}, u32[]{:S(2)}) copy-start(bf16[2048,1024]{1,0:T(8,128)(2,1)} %param.19) | copy-start | bytes 12582916
  0.0 6.1 %copy-start.11 = (f32[2048]{0:T(1024)S(1)}, f32[2048]{0:T(1024)}, u32[]{:S(2)}) copy-start(f32[2048]{0:T(1024)} %param.18) | copy-start | bytes 24580
  4.8 2.8 %slice-start.1 = ((s8[8388608]{0:T(1024)(128)(4,1)}), s8[4194304]{0:T(1024)(128)(4,1)S(1)}, s32[]{:S(2)}) async-start(s8[8388608]{0:T(1024)(128)(4,1)} %bitcast.44), calls=%async_computation.5 | async-start | bytes 8388608
  6.1 7.7 %copy-start.3 = (bf16[128,2048,8]{1,0,2:T(8,128)(2,1)}, bf16[128,2048,8]{1,0,2:T(8,128)(2,1)S(1)}, u32[]{:S(2)}) copy-start(bf16[128,2048,8]{1,0,2:T(8,128)(2,1)S(1)} %fusion.31) | copy-start | bytes 12582916
  13.8 56.0 %all-to-all-start = ((bf16[32,32,1024]{2,1,0:T(8,128)(2,1)}), bf16[32,32,1024]{2,1,0:T(8,128)(2,1)S(1)}, u32[]{:S(2)}, u32[]{:S(2)}) async-start(bf16[32,32,1024]{2,1,0:T(8,128)(2,1)} %bitcast.50), calls=%async_computation | async-start | bytes 4194304 | tf_op jit(solution)/shard_map/all_to_all | solution.py:215
  21.2 54.3 %copy-start.7 = (bf16[256,512]{1,0:T(8,128)(2,1)S(1)}, bf16[256,512]{1,0:T(8,128)(2,1)}, u32[]{:S(2)}) copy-start(bf16[256,512]{1,0:T(8,128)(2,1)} %constant.57.clone) | copy-start | bytes 786436
  21.2 54.3 %copy-start.8 = (bf16[256,512]{1,0:T(8,128)(2,1)S(1)}, bf16[256,512]{1,0:T(8,128)(2,1)}, u32[]{:S(2)}) copy-start(bf16[256,512]{1,0:T(8,128)(2,1)} %constant.56.clone) | copy-start | bytes 786436
  21.2 54.3 %copy-start.6 = (bf16[1,256,512]{2,1,0:T(8,128)(2,1)S(1)}, bf16[1,256,512]{2,1,0:T(8,128)(2,1)}, u32[]{:S(2)}) copy-start(bf16[1,256,512]{2,1,0:T(8,128)(2,1)} %constant.61) | copy-start | bytes 786436
  30.7 51.3 %copy-start.9 = (bf16[128,128,1]{1,0,2:T(8,128)(2,1)S(1)}, bf16[128,128,1]{1,0,2:T(8,128)(2,1)}, u32[]{:S(2)}) copy-start(bf16[128,128,1]{1,0,2:T(8,128)(2,1)} %constant.62) | copy-start | bytes 98308
  69.9 1.3 copy-start.5
  71.2 52.7 %all-to-all-start.1 = ((bf16[32,32,1024]{2,1,0:T(8,128)(2,1)}), bf16[32,32,1024]{2,1,0:T(8,128)(2,1)S(1)}, u32[]{:S(2)}, u32[]{:S(2)}) async-start(bf16[32,32,1024]{2,1,0:T(8,128)(2,1)} %bitcast.49), calls=%async_computation.1 | async-start | bytes 4194304 | tf_op jit(solution)/shard_map/all_to_all | solution.py:215
  75.4 6.6 %copy-start.2 = (bf16[1024,2048]{1,0:T(8,128)(2,1)S(1)}, bf16[1024,2048]{1,0:T(8,128)(2,1)}, u32[]{:S(2)}) copy-start(bf16[1024,2048]{1,0:T(8,128)(2,1)} %param.21) | copy-start | bytes 12582916
  123.9 1.3 copy-start.4
  125.3 52.7 %all-to-all-start.2 = ((bf16[32,8,32,128]{3,2,1,0:T(8,128)(2,1)}), bf16[32,8,32,128]{3,2,1,0:T(8,128)(2,1)S(1)}, u32[]{:S(2)}, u32[]{:S(2)}) async-start(bf16[32,8,32,128]{3,2,1,0:T(8,128)(2,1)} %shard_map.164), calls=%async_computation.2 | async-start | bytes 4194304 | tf_op jit(solution)/shard_map/all_to_all | solution.py:215
  178.0 4.2 %copy-start = (bf16[32,8,32,128]{3,2,1,0:T(8,128)(2,1)}, bf16[32,8,32,128]{3,2,1,0:T(8,128)(2,1)S(1)}, u32[]{:S(2)}) copy-start(bf16[32,8,32,128]{3,2,1,0:T(8,128)(2,1)S(1)} %all-to-all-done.2.r_ref) | copy-start | bytes 6291460
  178.0 52.8 %all-to-all-start.3 = ((bf16[32,8,32,128]{3,2,1,0:T(8,128)(2,1)}), bf16[32,8,32,128]{3,2,1,0:T(8,128)(2,1)}, u32[]{:S(2)}, u32[]{:S(2)}) async-start(bf16[32,8,32,128]{3,2,1,0:T(8,128)(2,1)} %shard_map.163), calls=%async_computation.3 | async-start | bytes 4194304 | tf_op jit(solution)/shard_map/all_to_all | solution.py:215
